TPU v7x, 128 devices: a whole 4x4x4 slice. The times are simulated.
128 devices in a mesh: ep: 16 (over z, x), tp: 8 (over y, core).
Axes of the slice: x: 4, y: 4, z: 4, core: 2. Of those that a mesh axis runs over, the one named last changes fastest.
Arguments:
- mix_tokens: bfloat16 [32768, 2048], P(('ep', 'tp')), may hold values from -40 to 40
- mix_gain: float32 [2048], replicated, may hold values from 0.1 to 1.9
- query_weight: bfloat16 [2048, 1024], replicated, may hold values from -0.125 to 0.125
- key_weight: bfloat16 [2048, 256], replicated, may hold values from -0.125 to 0.125
- value_weight: bfloat16 [2048, 256], replicated, may hold values from -0.125 to 0.125
- query_gain: float32 [64], replicated, may hold values from 0.5 to 40
- key_gain: float32 [64], replicated, may hold values from 0.1 to 1.9
- sink_logits: float32 [16], replicated, may hold values from 2 to 6
- out_weight: bfloat16 [1024, 2048], replicated, may hold values from -0.1875 to 0.1875
- moe_tokens: bfloat16 [16384, 2048], P(('ep', 'tp')), may hold values from -40 to 40
- moe_gain: float32 [2048], replicated, may hold values from 0.1 to 1.9
- routes: int32 [16384, 2], P(('ep', 'tp')), may hold values from 0 to 15, all different within a row; in each aligned block of 128 rows (0 to 127, 128 to 255, ...) at most 18 rows name the same one
- route_logits: float32 [16384, 2], P(('ep', 'tp')), may hold values from -6 to 6
- gate_weight: bfloat16 [16, 2048, 7168], P('ep', None, 'tp'), may hold values from -0.125 to 0.125
- up_weight: bfloat16 [16, 2048, 7168], P('ep', None, 'tp'), may hold values from -0.125 to 0.125
- down_weight: bfloat16 [16, 7168, 2048], P('ep', 'tp'), may hold values from -0.0625 to 0.0625
Outputs:
- mix_out: bfloat16 [32768, 2048], P(('ep', 'tp'))
- moe_out: bfloat16 [16384, 2048], P(('ep', 'tp'))
Inputs may be any that keep to these rules, and one draw needn't show every extreme that they name: `routes`: each row names 2 different experts. Of the rows of one device no expert is named more than 18 times, and in every draw some device names some expert exactly 18 times.
All inputs are finite; a program needn't handle non-finite values.
Results may differ from a plain program's by a relative error of at most 0.015.
The roundings to bfloat16 on the way count: a program that leaves them out, or rounds other values in their place, can miss the bound.
Values may be sent and summed in bfloat16 or wider, within the bound.
No kernel may reach another device: no remote copies, remote signals or barrier semaphores. Data moves between devices by JAX's collectives and lax.ppermute only.
A program may use at most 128 MiB of HBM per device.

v0:
```python
import jax
import jax.numpy as jnp
from jax import lax
from jax.sharding import PartitionSpec as P

WINDOW = 128
epsilon = 1e-06


def passed_along(block, axis, distance):
    devices = range(lax.axis_size(axis))
    route = [(i - distance, i) for i in devices if i - distance in devices]
    return lax.ppermute(block, axis, route)


def rms_scale(values, gain_vec):
    values = values.astype(jnp.float32)
    return (
        values * lax.rsqrt(jnp.mean(values * values, axis=-1, keepdims=True) + epsilon) * gain_vec
    )


def route_slots(routes, experts, capacity):
    flat_ids = routes.reshape(-1)
    onehot = (flat_ids[:, None] == jnp.arange(experts, dtype=jnp.int32)[None, :]).astype(jnp.int32)
    before = jnp.cumsum(onehot, axis=0) - onehot
    slot_ids = jnp.sum(before * onehot, axis=1)
    return (flat_ids * capacity + slot_ids).reshape(routes.shape)


def window_attention(queries, key_ext, value_ext, sink_logits, first_pos):
    row_count = queries.shape[0]
    window_rows = key_ext.shape[0] - row_count
    blocks = row_count // window_rows
    kv_heads = key_ext.shape[1]
    group_size = queries.shape[1] // kv_heads
    head_dim = queries.shape[2]
    query_blk = queries.reshape(blocks, window_rows, kv_heads, group_size, head_dim)

    def pair_up(source):
        lower = source[:row_count].reshape(blocks, window_rows, kv_heads, head_dim)
        upper = source[window_rows:].reshape(blocks, window_rows, kv_heads, head_dim)
        return jnp.concatenate([lower, upper], axis=1)

    key_blk = pair_up(key_ext)
    value_blk = pair_up(value_ext)
    scores = jnp.einsum(
        "bqkgd,bskd->bkgqs", query_blk, key_blk, preferred_element_type=jnp.float32
    ) * head_dim ** (-0.5)
    query_pos = jnp.arange(window_rows, dtype=jnp.int32)[:, None] + window_rows
    key_pos = jnp.arange(2 * window_rows, dtype=jnp.int32)[None, :]
    pos_gap = query_pos - key_pos
    block_start = first_pos + jnp.arange(blocks, dtype=jnp.int32) * window_rows - window_rows
    key_global = block_start[:, None] + jnp.arange(2 * window_rows, dtype=jnp.int32)[None, :]
    visible = ((pos_gap >= 0) & (pos_gap <= window_rows))[None] & (key_global >= 0)[:, None, :]
    scores = jnp.where(visible[:, None, None], scores, -jnp.inf)
    sink_col = sink_logits.reshape(kv_heads, group_size)[None, :, :, None, None]
    row_top = jnp.maximum(jnp.max(scores, axis=-1, keepdims=True), sink_col)
    weights = jnp.exp(scores - row_top)
    denom_sum = jnp.sum(weights, axis=-1, keepdims=True) + jnp.exp(sink_col - row_top)
    attn_prob = (weights / denom_sum).astype(jnp.bfloat16)
    mixed_out = jnp.einsum(
        "bkgqs,bskd->bqkgd", attn_prob, value_blk, preferred_element_type=jnp.float32
    )
    return mixed_out.astype(jnp.bfloat16).reshape(row_count, -1)


def body(
    mix_tokens,
    mix_gain,
    query_weight,
    key_weight,
    value_weight,
    query_gain,
    key_gain,
    sink_logits,
    out_weight,
    moe_tokens,
    moe_gain,
    routes,
    route_logits,
    gate_weight,
    up_weight,
    down_weight,
):
    row_count = mix_tokens.shape[0]
    head_count = sink_logits.shape[0]
    head_dim = query_gain.shape[0]
    kv_heads = key_weight.shape[1] // head_dim
    normed = rms_scale(mix_tokens, mix_gain).astype(jnp.bfloat16)
    queries = jnp.dot(normed, query_weight, preferred_element_type=jnp.float32)
    queries = rms_scale(queries.reshape(row_count, head_count, head_dim), query_gain).astype(
        jnp.bfloat16
    )
    key_rows = jnp.dot(normed, key_weight, preferred_element_type=jnp.float32)
    key_rows = rms_scale(key_rows.reshape(row_count, kv_heads, head_dim), key_gain).astype(
        jnp.bfloat16
    )
    values = jnp.dot(normed, value_weight, preferred_element_type=jnp.float32).astype(jnp.bfloat16)
    values = values.reshape(row_count, kv_heads, head_dim)
    rim_keys, rim_values = passed_along(
        (key_rows[row_count - WINDOW :], values[row_count - WINDOW :]), ("ep", "tp"), 1
    )
    key_ext = jnp.concatenate([rim_keys, key_rows], axis=0)
    value_ext = jnp.concatenate([rim_values, values], axis=0)
    first_pos = lax.axis_index(("ep", "tp")) * row_count
    attended = window_attention(queries, key_ext, value_ext, sink_logits, first_pos)
    mix_out = jnp.dot(attended, out_weight, preferred_element_type=jnp.float32).astype(jnp.bfloat16)
    moe_rows = moe_tokens.shape[0]
    model_width = moe_tokens.shape[1]
    experts = lax.axis_size("ep")
    capacity = (9 * moe_rows * routes.shape[1] + 8 * experts - 1) // (8 * experts)
    moe_normed = rms_scale(moe_tokens, moe_gain).astype(jnp.bfloat16)
    targets = route_slots(routes, experts, capacity)
    slot_ids = jnp.arange(experts * capacity, dtype=jnp.int32)
    pick_rows = jnp.sum(
        (targets[None, :, :] == slot_ids[:, None, None]).astype(jnp.bfloat16), axis=2
    )
    packed = jnp.dot(pick_rows, moe_normed, preferred_element_type=jnp.float32).astype(jnp.bfloat16)
    reached = lax.all_to_all(
        packed.reshape(experts, 1, capacity, model_width),
        "ep",
        split_axis=0,
        concat_axis=0,
        tiled=True,
    )
    arrived_grid = lax.all_gather(reached, "tp", axis=1, tiled=True)
    gate_act = jnp.einsum(
        "etcd,df->tecf", arrived_grid, gate_weight[0], preferred_element_type=jnp.float32
    )
    up_act = jnp.einsum(
        "etcd,df->tecf", arrived_grid, up_weight[0], preferred_element_type=jnp.float32
    )
    hidden = (jax.nn.silu(gate_act) * up_act).astype(jnp.bfloat16)
    own_rows = lax.psum_scatter(
        jnp.einsum(
            "tecf,fd->tecd", hidden, down_weight[0], preferred_element_type=jnp.float32
        ).astype(jnp.bfloat16),
        "tp",
        scatter_dimension=0,
        tiled=True,
    ).astype(jnp.float32)
    returned = lax.all_to_all(
        own_rows[0].astype(jnp.bfloat16), "ep", split_axis=0, concat_axis=0, tiled=True
    )
    results = returned.reshape(experts * capacity, model_width)
    gate_probs = jax.nn.softmax(route_logits, axis=-1).astype(jnp.bfloat16)
    combine = jnp.where(
        targets[:, :, None] == slot_ids[None, None, :],
        gate_probs[:, :, None],
        jnp.zeros((), jnp.bfloat16),
    )
    combine = jnp.sum(combine, axis=1)
    moe_out = jnp.dot(combine, results, preferred_element_type=jnp.float32).astype(jnp.bfloat16)
    return (mix_out, moe_out)


def solution(mesh):
    placed = (
        P(("ep", "tp"), None),
        P(),
        P(),
        P(),
        P(),
        P(),
        P(),
        P(),
        P(),
        P(("ep", "tp"), None),
        P(),
        P(("ep", "tp"), None),
        P(("ep", "tp"), None),
        P("ep", None, "tp"),
        P("ep", None, "tp"),
        P("ep", "tp", None),
    )
    return jax.shard_map(
        body,
        mesh=mesh,
        in_specs=placed,
        out_specs=(P(("ep", "tp"), None), P(("ep", "tp"), None)),
        check_vma=False,
    )
```

profile of v0, /device:TPU:8, one launch (start us, length us, event | category | flops | bytes accessed | tf_op | source)
XLA Modules:
  0.0 282.8 jit_solution(16053804923481000589)
XLA Ops:
  7.2 0.9 copy.71
  8.1 0.1 eq.55
  8.2 0.1 eq.51
  8.4 0.6 reduce-window.6
  9.0 0.2 slice_reduce_fusion
  9.2 0.1 fusion.44
  9.3 0.1 reduce_sum.94
  9.5 0.7 multiply_add_fusion
  10.3 1.2 fusion.17
  11.5 2.6 convolution_convert_fusion.1
  14.1 1.4 reshape.199
  15.5 30.5 %all_to_all.10 = bf16[16,1,18,2048]{3,2,1,0:T(8,128)(2,1)} all-to-all(bf16[16,1,18,2048]{3,2,1,0:T(8,128)(2,1)S(1)} %bitcast.129), channel_id=1, replica_groups=mesh['ep'=16,'tp'=8] {'ep'}, dimensions={0} | all-to-all | bytes 2359296 | tf_op jit(solution)/shard_map/all_to_all | solution.py:120
  46.2 64.4 %all-gather.2.cloned.1.call-done = bf16[16,8,18,2048]{3,2,1,0:T(8,128)(2,1)} async-done(((bf16[16,1,18,2048]{3,2,1,0:T(8,128)(2,1)}), bf16[16,8,18,2048]{3,2,1,0:T(8,128)(2,1)}) %all-gather.2.cloned.1.call-update) | async-done | bytes 9437200 | tf_op jit(solution)/shard_map/all_gather | solution.py:127
  110.5 18.8 %fusion.7 = f32[16,8,18,896]{3,2,1,0:T(8,128)} fusion(bf16[16,8,18,2048]{3,2,1,0:T(8,128)(2,1)} %all-gather.2.cloned.1.call-done, bf16[1,2048,896]{2,1,0:T(8,128)(2,1)} %param.30), kind=kOutput, calls=%fused_computation.14 | convolution fusion | flops 8455716864 | bytes 21364736 | tf_op jit(solution)/shard_map/etcd,df->tecf/dot_general | solution.py:131
  129.3 18.7 %fusion = bf16[8,16,18,896]{3,2,0,1:T(8,128)(2,1)} fusion(f32[16,8,18,896]{3,2,1,0:T(8,128)} %fusion.7, bf16[16,8,18,2048]{3,2,1,0:T(8,128)(2,1)S(1)} %copy-done.6, bf16[1,2048,896]{2,1,0:T(8,128)(2,1)} %param.29), kind=kOutput, calls=%fused_computation.1 | convolution fusion | flops 8468103168 | bytes 25493504 | tf_op jit(solution)/shard_map/etcd,df->tecf/dot_general | solution.py:128
  148.0 19.0 %convolution_convert_fusion = bf16[8,16,18,2048]{3,2,1,0:T(8,128)(2,1)} fusion(bf16[8,16,18,896]{3,2,0,1:T(8,128)(2,1)} %fusion, bf16[1,896,2048]{2,1,0:T(8,128)(2,1)} %param.31), kind=kOutput, calls=%fused_computation.7 | convolution fusion | flops 8460435456 | bytes 17235968 | tf_op jit(solution)/shard_map/tecf,fd->tecd/dot_general | solution.py:136
  167.1 1.2 copy-done.2
  168.3 0.3 fusion.11
  168.6 0.7 multiply_reduce_fusion
  169.4 0.6 slice.29
  170.0 2.1 collective-permute-start.1
  172.1 0.7 convolution_convert_fusion.4
  172.9 0.7 slice.28
  173.5 3.0 %collective-permute-start = (bf16[128,4,64]{0,2,1:T(8,128)(2,1)}, bf16[128,4,64]{0,2,1:T(8,128)(2,1)}, u32[]{:S(2)}, u32[]{:S(2)}) collective-permute-start(bf16[128,4,64]{0,2,1:T(8,128)(2,1)} %bitcast), channel_id=1, source_target_pairs={{0,1},{1,2},{2,3},{3,4},{4,5},{5,6},{6,7},{7,8},{8,9},{9,10},{10,1... | collective-permute-start | bytes 196616 | tf_op jit(solution)/shard_map/ppermute | solution.py:13
  176.5 0.1 reshape.195
  176.6 0.7 reshape_reshape.3
  177.3 5.1 %fusion.57 = (f32[256,1024]{1,0:T(8,128)}, f32[256,1024]{1,0:T(8,128)}) fusion(bf16[2048,1024]{1,0:T(8,128)(2,1)} %param.18, bf16[256,2048]{1,0:T(8,128)(2,1)S(1)} %copy-done.2, f32[2048]{0:T(1024)S(1)} %copy-done.9, f32[256]{0:T(256)S(1)} %add_rsqrt_fusion.2), kind=kOutput, calls=%fused_computation.100 | convolution fusion | flops 1076101120 | bytes 7349248 | tf_op jit(solution)/shard_map/dot_general | solution.py:91
  182.5 1.6 copy.66
  184.1 0.5 reshape.196
  184.6 1.6 copy.67
  186.3 0.7 max.20
  187.0 0.9 copy.63
  188.2 0.1 broadcast_and_fusion
  188.3 0.8 fusion.34
  189.1 1.3 multiply_convert_fusion
  190.4 0.9 copy_bitcast_fusion
  191.3 0.9 copy_bitcast_fusion.1
  192.2 0.8 fusion.10
  193.1 1.9 copy-done.1
  195.0 1.0 fusion.5
  196.0 42.9 %reduce-scatter.2.cloned.1.call-done = bf16[1,16,18,2048]{3,2,1,0:T(8,128)(2,1)} async-done(((bf16[8,16,18,2048]{3,2,1,0:T(8,128)(2,1)}), bf16[1,16,18,2048]{3,2,1,0:T(8,128)(2,1)}) %reduce-scatter.2.cloned.1.call-update) | async-done | bytes 1179664 | tf_op jit(solution)/shard_map/reduce_scatter | solution.py:135
  238.9 7.2 %all-to-all-start.1 = ((bf16[16,18,2048]{2,1,0:T(8,128)(2,1)}), bf16[16,18,2048]{2,1,0:T(8,128)(2,1)S(1)}, u32[]{:S(2)}, u32[]{:S(2)}) async-start(bf16[16,18,2048]{2,1,0:T(8,128)(2,1)} %bitcast.130), calls=%async_computation.2 | async-start | bytes 3145728 | tf_op jit(solution)/shard_map/all_to_all | solution.py:143
  246.1 3.5 %fusion.16 = bf16[2,128,4,4,64]{1,4,3,2,0:T(8,128)(2,1)S(1)} fusion(f32[2,4,256,128,4]{3,2,4,1,0:T(8,128)} %copy-done.1, f32[2,4,4,128]{3,2,1,0:T(4,128)S(1)} %exponential_add_fusion, f32[2,4,4,128]{3,2,1,0:T(4,128)S(1)} %broadcast_maximum_fusion, pred[2,128,256]{1,2,0:T(8,128)(4,1)S(1)} %broadcast_and_fusion, bf16[2,128,4,64]{1,3,2,0:T(8,128)(2,1)S(1)} %copy.63, ...), kind=kOutput, calls=%fused_computation.30 | convolution fusion | flops 140247040 | bytes 5079040 | tf_op jit(solution)/shard_map/bkgqs,bskd->bqkgd/dot_general | solution.py:62
  249.6 0.5 copy.70
  250.2 2.3 convolution_convert_fusion.2
  252.4 19.8 %all-to-all-done.1 = bf16[16,18,2048]{2,1,0:T(8,128)(2,1)S(1)} async-done(((bf16[16,18,2048]{2,1,0:T(8,128)(2,1)}), bf16[16,18,2048]{2,1,0:T(8,128)(2,1)S(1)}, u32[]{:S(2)}, u32[]{:S(2)}) %all-to-all-start.1) | async-done | bytes 1179680 | tf_op jit(solution)/shard_map/all_to_all | solution.py:143
  272.2 1.2 reshape.200
  273.4 2.5 convolution_convert_fusion.3
  (46 shorter events, 0.9 us)
Async XLA Ops:
  7.2 161.4 %copy-start = (bf16[2048,256]{1,0:T(8,128)(2,1)S(1)}, bf16[2048,256]{1,0:T(8,128)(2,1)}, u32[]{:S(2)}) copy-start(bf16[2048,256]{1,0:T(8,128)(2,1)} %param.19) | copy-start | bytes 3145732
  7.2 103.3 %all-gather.2.cloned.1.call-start = ((), (), s32[]{:S(2)}) async-start(), calls=%async_computation.3 | async-start | bytes 14155776 | tf_op jit(solution)/shard_map/all_gather | solution.py:127
  46.1 192.8 %reduce-scatter.2.cloned.1.call-start = ((), (), s32[]{:S(2)}) async-start(), calls=%async_computation.4 | async-start | bytes 14155776 | tf_op jit(solution)/shard_map/reduce_scatter | solution.py:135
  110.5 18.8 %copy-start.6 = (bf16[16,8,18,2048]{3,2,1,0:T(8,128)(2,1)S(1)}, bf16[16,8,18,2048]{3,2,1,0:T(8,128)(2,1)}, u32[]{:S(2)}) copy-start(bf16[16,8,18,2048]{3,2,1,0:T(8,128)(2,1)} %all-gather.2.cloned.1.call-done) | copy-start | bytes 28311556
  167.0 1.2 copy-start.2
  167.0 1.5 copy-start.9
  167.0 2.2 copy-start.5
  168.3 3.9 %copy-start.8 = (bf16[2048,256]{1,0:T(8,128)(2,1)S(1)}, bf16[2048,256]{1,0:T(8,128)(2,1)}, u32[]{:S(2)}) copy-start(bf16[2048,256]{1,0:T(8,128)(2,1)} %param.20) | copy-start | bytes 3145732
  170.0 20.4 %collective-permute-start.1 = (bf16[128,4,64]{0,2,1:T(8,128)(2,1)}, bf16[128,4,64]{0,2,1:T(8,128)(2,1)}, u32[]{:S(2)}, u32[]{:S(2)}) collective-permute-start(bf16[128,4,64]{0,2,1:T(8,128)(2,1)} %slice.29), channel_id=1, source_target_pairs={{0,1},{1,2},{2,3},{3,4},{4,5},{5,6},{6,7},{7,8},{8,9},{9,10},{10,1... | collective-permute-start | bytes 196616 | tf_op jit(solution)/shard_map/ppermute | solution.py:13
  172.8 9.6 %copy-start.3 = (bf16[256,256]{0,1:T(8,128)(2,1)}, bf16[256,256]{0,1:T(8,128)(2,1)S(1)}, u32[]{:S(2)}) copy-start(bf16[256,256]{0,1:T(8,128)(2,1)S(1)} %convolution_convert_fusion.4) | copy-start | bytes 393220
  173.5 17.8 %collective-permute-start = (bf16[128,4,64]{0,2,1:T(8,128)(2,1)}, bf16[128,4,64]{0,2,1:T(8,128)(2,1)}, u32[]{:S(2)}, u32[]{:S(2)}) collective-permute-start(bf16[128,4,64]{0,2,1:T(8,128)(2,1)} %bitcast), channel_id=1, source_target_pairs={{0,1},{1,2},{2,3},{3,4},{4,5},{5,6},{6,7},{7,8},{8,9},{9,10},{10,1... | collective-permute-start | bytes 196616 | tf_op jit(solution)/shard_map/ppermute | solution.py:13
  182.5 5.5 %copy-start.4 = (f32[128,2]{0,1:T(2,128)S(1)}, f32[128,2]{0,1:T(2,128)}, u32[]{:S(2)}) copy-start(f32[128,2]{0,1:T(2,128)} %param.28) | copy-start | bytes 3076
  193.0 2.0 copy-start.1
  238.9 33.3 %all-to-all-start.1 = ((bf16[16,18,2048]{2,1,0:T(8,128)(2,1)}), bf16[16,18,2048]{2,1,0:T(8,128)(2,1)S(1)}, u32[]{:S(2)}, u32[]{:S(2)}) async-start(bf16[16,18,2048]{2,1,0:T(8,128)(2,1)} %bitcast.130), calls=%async_computation.2 | async-start | bytes 3145728 | tf_op jit(solution)/shard_map/all_to_all | solution.py:143
  246.1 4.1 %copy-start.7 = (bf16[1024,2048]{1,0:T(8,128)(2,1)S(1)}, bf16[1024,2048]{1,0:T(8,128)(2,1)}, u32[]{:S(2)}) copy-start(bf16[1024,2048]{1,0:T(8,128)(2,1)} %param.24) | copy-start | bytes 12582916
Sparse Core Ops, SparseCore 0:
  46.2 64.2 all-gather.1
  167.2 71.6 reduce-scatter.1
where the time goes:
time: 283 us
  waiting for transfers between devices  127 us (45%)
  matrix products  74.7 us (26%)
  blocking collectives  30.5 us (11%)
  local copies, waits for them, and re-layouts  15.3 us (5%)
  between operations  14.4 us (5%)
  starting transfers between devices  12.3 us (4%)
  other arithmetic  8.43 us (3%)
    all_gather x1, waiting for transfers between devices, body(): arrived_grid = lax.all_gather(reached, 'tp', axis=1, tiled=True)  64.4 us
    reduce_scatter x1, waiting for transfers between devices, body(): lax.psum_scatter(jnp.einsum('tecf,fd->tecd', hidden, down_weight[0], pref...  42.9 us
    all_to_all x1, blocking collectives, body(): lax.all_to_all(packed.reshape(experts, 1, capacity, model_width), 'ep', s...  30.5 us
    all_to_all x1, waiting for transfers between devices, body(): lax.all_to_all(own_rows[0].astype(jnp.bfloat16), 'ep', split_axis=0, conc...  19.8 us
    dot_general x1, matrix products, body(): jnp.einsum('tecf,fd->tecd', hidden, down_weight[0], preferred_element_typ...  19 us
    dot_general x1, matrix products, body(): jnp.einsum('etcd,df->tecf', arrived_grid, up_weight[0], preferred_element...  18.8 us
    dot_general x1, matrix products, body(): jnp.einsum('etcd,df->tecf', arrived_grid, gate_weight[0], preferred_eleme...  18.7 us
    all_to_all x1, starting transfers between devices, body(): lax.all_to_all(own_rows[0].astype(jnp.bfloat16), 'ep', split_axis=0, conc...  7.15 us
  transfers between devices with their start and end apart: 5, of which 3 were waited for; matrix products, arithmetic and copies ran while one was open for 9% of the time, Pallas kernels for 0%

commit v1 on v0

--- a/solution.py
+++ b/solution.py
@@ -124,7 +124,8 @@
         concat_axis=0,
         tiled=True,
     )
-    arrived_grid = lax.all_gather(reached, "tp", axis=1, tiled=True)
+    outgoing = jnp.stack([reached] * lax.axis_size("tp"))
+    arrived_grid = jnp.concatenate(lax.all_to_all(outgoing, "tp", 0, 0), axis=1)
     gate_act = jnp.einsum(
         "etcd,df->tecf", arrived_grid, gate_weight[0], preferred_element_type=jnp.float32
     )

time: 283 us -> 355 us (1.25); the launches traced: 283 us -> 351 us
  blocking collectives: 30.5 us -> 142 us
  waiting for transfers between devices: 127 us -> 59.9 us
  matrix products: 74.7 us -> 94.7 us
  local copies, waits for them, and re-layouts: 15.3 us -> 20.8 us
    all_to_all x0 -> x1, blocking collectives: none -> 111 us  [body(): arrived_grid = jnp.concatenate(lax.all_to_all(outgoing, 'tp', 0, 0), axis=1)]
    all_gather x1 -> x0, waiting for transfers between devices: 64.4 us -> none  [body(): arrived_grid = lax.all_gather(reached, 'tp', axis=1, tiled=True)]
    dot_general x1, matrix products: 18.7 us -> 30.8 us  [body(): jnp.einsum('etcd,df->tecf', arrived_grid, gate_weight[0], preferred_eleme...]
    dot_general x1, matrix products: 18.8 us -> 27.6 us  [body(): jnp.einsum('etcd,df->tecf', arrived_grid, up_weight[0], preferred_element...]
    unnamed x21 -> x27, local copies, waits for them, and re-layouts: 3.97 us -> 7.56 us
  transfers between devices with their start and end apart: 5 -> 4, of which waited for: 3 -> 2; matrix products, arithmetic and copies ran while one was open for 9% -> 8% of each run, Pallas kernels for 0% -> 0%
where the time goes in v1:
time: 355 us; the launch traced here: 351 us
  blocking collectives  142 us (40%)
  matrix products  94.7 us (27%)
  waiting for transfers between devices  59.9 us (17%)
  local copies, waits for them, and re-layouts  20.8 us (6%)
  between operations  14.6 us (4%)
  starting transfers between devices  10.6 us (3%)
  other arithmetic  8.44 us (2%)
    all_to_all x1, blocking collectives, body(): arrived_grid = jnp.concatenate(lax.all_to_all(outgoing, 'tp', 0, 0), axis=1)  111 us
    reduce_scatter x1, waiting for transfers between devices, body(): lax.psum_scatter(jnp.einsum('tecf,fd->tecd', hidden, down_weight[0], pref...  40.1 us
    dot_general x1, matrix products, body(): jnp.einsum('etcd,df->tecf', arrived_grid, gate_weight[0], preferred_eleme...  30.8 us
    all_to_all x1, blocking collectives, body(): lax.all_to_all(packed.reshape(experts, 1, capacity, model_width), 'ep', s...  30.4 us
    dot_general x1, matrix products, body(): jnp.einsum('etcd,df->tecf', arrived_grid, up_weight[0], preferred_element...  27.6 us
    all_to_all x1, waiting for transfers between devices, body(): lax.all_to_all(own_rows[0].astype(jnp.bfloat16), 'ep', split_axis=0, conc...  19.8 us
    dot_general x1, matrix products, body(): jnp.einsum('tecf,fd->tecd', hidden, down_weight[0], preferred_element_typ...  18.4 us
    unnamed x27, local copies, waits for them, and re-layouts  7.56 us
  transfers between devices with their start and end apart: 4, of which 2 were waited for; matrix products, arithmetic and copies ran while one was open for 8% of the time, Pallas kernels for 0%

profile of v1, /device:TPU:8, one launch (start us, length us, event | category | flops | bytes accessed | tf_op | source)
XLA Modules:
  0.0 350.8 jit_solution(5487714742276406490)
XLA Ops:
  7.2 0.9 copy.90
  8.1 0.1 eq.55
  8.2 0.1 eq.51
  8.4 0.6 reduce-window.6
  9.0 0.2 slice_reduce_fusion
  9.3 0.1 reduce_sum.94
  9.5 0.7 multiply_add_fusion
  10.3 1.2 fusion.24
  11.5 2.6 convolution_convert_fusion.1
  14.1 1.4 reshape.208
  15.5 30.4 %all_to_all.18 = bf16[16,1,18,2048]{3,2,1,0:T(8,128)(2,1)S(1)} all-to-all(bf16[16,1,18,2048]{3,2,1,0:T(8,128)(2,1)S(1)} %bitcast.137), channel_id=1, replica_groups=mesh['ep'=16,'tp'=8] {'ep'}, dimensions={0} | all-to-all | bytes 2359296 | tf_op jit(solution)/shard_map/all_to_all | solution.py:120
  46.0 0.7 copy.95
  46.6 1.2 stack.2
  47.9 111.4 %all_to_all.19 = bf16[8,16,1,18,2048]{4,1,3,2,0:T(8,128)(2,1)S(1)} all-to-all(bf16[8,16,1,18,2048]{4,1,3,2,0:T(8,128)(2,1)S(1)} %stack.2), channel_id=1, replica_groups=mesh['ep'=16,'tp'=8] {'tp'}, dimensions={0} | all-to-all | bytes 18874368 | tf_op jit(solution)/shard_map/all_to_all | solution.py:128
  159.2 3.6 %copy-done.1 = bf16[8,16,1,18,2048]{4,1,3,2,0:T(8,128)(2,1)} copy-done((bf16[8,16,1,18,2048]{4,1,3,2,0:T(8,128)(2,1)}, bf16[8,16,1,18,2048]{4,1,3,2,0:T(8,128)(2,1)S(1)}, u32[]{:S(2)}) %copy-start.1) | copy-done | bytes 9437208
  162.8 27.6 %fusion = f32[16,8,18,896]{3,2,1,0:T(8,128)} fusion(bf16[8,16,1,18,2048]{4,1,3,2,0:T(8,128)(2,1)S(1)} %all_to_all.19, bf16[1,2048,896]{2,1,0:T(8,128)(2,1)S(1)} %copy-done.8), kind=kOutput, calls=%fused_computation | convolution fusion | flops 8455716864 | bytes 21364736 | tf_op jit(solution)/shard_map/etcd,df->tecf/dot_general | solution.py:132
  190.4 30.8 %fusion.6 = bf16[8,16,18,896]{3,2,0,1:T(8,128)(2,1)} fusion(f32[16,8,18,896]{3,2,1,0:T(8,128)} %fusion, bf16[8,16,1,18,2048]{4,1,3,2,0:T(8,128)(2,1)} %copy-done.1, bf16[1,2048,896]{2,1,0:T(8,128)(2,1)S(1)} %copy-done.9), kind=kOutput, calls=%fused_computation.7 | convolution fusion | flops 8468103168 | bytes 25493504 | tf_op jit(solution)/shard_map/etcd,df->tecf/dot_general | solution.py:129
  221.2 18.4 %convolution_convert_fusion = bf16[8,16,18,2048]{3,2,1,0:T(8,128)(2,1)} fusion(bf16[8,16,18,896]{3,2,0,1:T(8,128)(2,1)} %fusion.6, bf16[1,896,2048]{2,1,0:T(8,128)(2,1)S(1)} %copy-done.10), kind=kOutput, calls=%fused_computation.13 | convolution fusion | flops 8460435456 | bytes 17235968 | tf_op jit(solution)/shard_map/tecf,fd->tecd/dot_general | solution.py:137
  239.6 1.2 copy-done.3
  240.8 0.3 fusion.18
  241.1 0.7 multiply_reduce_fusion
  241.9 0.6 slice.29
  242.6 1.9 collective-permute-start.1
  244.5 0.7 convolution_convert_fusion.4
  245.2 0.7 slice.28
  245.9 1.9 collective-permute-start
  247.9 0.7 reshape_reshape.3
  248.6 4.9 %fusion.64 = (f32[256,1024]{1,0:T(8,128)}, f32[256,1024]{1,0:T(8,128)}) fusion(bf16[2048,1024]{1,0:T(8,128)(2,1)} %param.18, bf16[256,2048]{1,0:T(8,128)(2,1)S(1)} %copy-done.3, f32[2048]{0:T(1024)S(1)} %copy-done.12, f32[256]{0:T(256)S(1)} %add_rsqrt_fusion.2), kind=kOutput, calls=%fused_computation.105 | convolution fusion | flops 1076101120 | bytes 7349248 | tf_op jit(solution)/shard_map/dot_general | solution.py:91
  253.5 1.6 copy.85
  255.1 0.5 reshape.205
  255.6 1.6 copy.86
  257.4 0.7 max.20
  258.1 0.9 copy.82
  259.4 0.7 fusion.41
  260.2 1.3 multiply_convert_fusion
  261.5 0.9 copy_bitcast_fusion
  262.4 0.9 copy_bitcast_fusion.1
  263.3 0.8 fusion.17
  264.2 1.9 copy-done.2
  266.1 1.0 fusion.13
  267.1 40.1 %reduce-scatter.2.cloned.1.call-done = bf16[1,16,18,2048]{3,2,1,0:T(8,128)(2,1)} async-done(((bf16[8,16,18,2048]{3,2,1,0:T(8,128)(2,1)}), bf16[1,16,18,2048]{3,2,1,0:T(8,128)(2,1)}) %reduce-scatter.2.cloned.1.call-update) | async-done | bytes 1179664 | tf_op jit(solution)/shard_map/reduce_scatter | solution.py:136
  307.1 6.7 %all-to-all-start.2 = ((bf16[16,18,2048]{2,1,0:T(8,128)(2,1)}), bf16[16,18,2048]{2,1,0:T(8,128)(2,1)S(1)}, u32[]{:S(2)}, u32[]{:S(2)}) async-start(bf16[16,18,2048]{2,1,0:T(8,128)(2,1)} %bitcast.139), calls=%async_computation.3 | async-start | bytes 3145728 | tf_op jit(solution)/shard_map/all_to_all | solution.py:144
  313.9 3.5 %fusion.23 = bf16[2,128,4,4,64]{1,4,3,2,0:T(8,128)(2,1)S(1)} fusion(f32[2,4,256,128,4]{3,2,4,1,0:T(8,128)} %copy-done.2, f32[2,4,4,128]{3,2,1,0:T(4,128)S(1)} %exponential_add_fusion, f32[2,4,4,128]{3,2,1,0:T(4,128)S(1)} %broadcast_maximum_fusion, pred[2,128,256]{1,2,0:T(8,128)(4,1)S(1)} %broadcast_and_fusion, bf16[2,128,4,64]{1,3,2,0:T(8,128)(2,1)S(1)} %copy.82, ...), kind=kOutput, calls=%fused_computation.35 | convolution fusion | flops 140247040 | bytes 5079040 | tf_op jit(solution)/shard_map/bkgqs,bskd->bqkgd/dot_general | solution.py:62
  317.4 0.5 copy.89
  318.0 2.3 convolution_convert_fusion.2
  320.2 19.8 %all-to-all-done.2 = bf16[16,18,2048]{2,1,0:T(8,128)(2,1)S(1)} async-done(((bf16[16,18,2048]{2,1,0:T(8,128)(2,1)}), bf16[16,18,2048]{2,1,0:T(8,128)(2,1)S(1)}, u32[]{:S(2)}, u32[]{:S(2)}) %all-to-all-start.2) | async-done | bytes 1179680 | tf_op jit(solution)/shard_map/all_to_all | solution.py:144
  340.0 1.2 reshape.211
  341.2 2.5 convolution_convert_fusion.3
  (52 shorter events, 1.2 us)
Async XLA Ops:
  7.2 234.0 %copy-start = (bf16[2048,256]{1,0:T(8,128)(2,1)S(1)}, bf16[2048,256]{1,0:T(8,128)(2,1)}, u32[]{:S(2)}) copy-start(bf16[2048,256]{1,0:T(8,128)(2,1)} %param.19) | copy-start | bytes 3145732
  7.2 300.0 %reduce-scatter.2.cloned.1.call-start = ((), (), s32[]{:S(2)}) async-start(), calls=%async_computation.4 | async-start | bytes 14155776 | tf_op jit(solution)/shard_map/reduce_scatter | solution.py:136
  47.9 114.9 %copy-start.8 = (bf16[1,2048,896]{2,1,0:T(8,128)(2,1)S(1)}, bf16[1,2048,896]{2,1,0:T(8,128)(2,1)}, u32[]{:S(2)}) copy-start(bf16[1,2048,896]{2,1,0:T(8,128)(2,1)} %param.30) | copy-start | bytes 11010052
  159.2 3.6 %copy-start.1 = (bf16[8,16,1,18,2048]{4,1,3,2,0:T(8,128)(2,1)}, bf16[8,16,1,18,2048]{4,1,3,2,0:T(8,128)(2,1)S(1)}, u32[]{:S(2)}) copy-start(bf16[8,16,1,18,2048]{4,1,3,2,0:T(8,128)(2,1)S(1)} %all_to_all.19) | copy-start | bytes 28311556
  162.8 27.6 %copy-start.9 = (bf16[1,2048,896]{2,1,0:T(8,128)(2,1)S(1)}, bf16[1,2048,896]{2,1,0:T(8,128)(2,1)}, u32[]{:S(2)}) copy-start(bf16[1,2048,896]{2,1,0:T(8,128)(2,1)} %param.29) | copy-start | bytes 11010052
  190.4 30.8 %copy-start.10 = (bf16[1,896,2048]{2,1,0:T(8,128)(2,1)S(1)}, bf16[1,896,2048]{2,1,0:T(8,128)(2,1)}, u32[]{:S(2)}) copy-start(bf16[1,896,2048]{2,1,0:T(8,128)(2,1)} %param.31) | copy-start | bytes 11010052
  239.6 1.2 copy-start.3
  239.6 1.5 copy-start.12
  239.6 2.2 copy-start.6
  240.8 3.7 %copy-start.11 = (bf16[2048,256]{1,0:T(8,128)(2,1)S(1)}, bf16[2048,256]{1,0:T(8,128)(2,1)}, u32[]{:S(2)}) copy-start(bf16[2048,256]{1,0:T(8,128)(2,1)} %param.20) | copy-start | bytes 3145732
  242.6 19.0 %collective-permute-start.1 = (bf16[128,4,64]{0,2,1:T(8,128)(2,1)}, bf16[128,4,64]{0,2,1:T(8,128)(2,1)}, u32[]{:S(2)}, u32[]{:S(2)}) collective-permute-start(bf16[128,4,64]{0,2,1:T(8,128)(2,1)} %slice.29), channel_id=1, source_target_pairs={{0,1},{1,2},{2,3},{3,4},{4,5},{5,6},{6,7},{7,8},{8,9},{9,10},{10,1... | collective-permute-start | bytes 196616 | tf_op jit(solution)/shard_map/ppermute | solution.py:13
  245.2 8.3 %copy-start.4 = (bf16[256,256]{0,1:T(8,128)(2,1)}, bf16[256,256]{0,1:T(8,128)(2,1)S(1)}, u32[]{:S(2)}) copy-start(bf16[256,256]{0,1:T(8,128)(2,1)S(1)} %convolution_convert_fusion.4) | copy-start | bytes 393220
  245.9 16.5 %collective-permute-start = (bf16[128,4,64]{0,2,1:T(8,128)(2,1)}, bf16[128,4,64]{0,2,1:T(8,128)(2,1)}, u32[]{:S(2)}, u32[]{:S(2)}) collective-permute-start(bf16[128,4,64]{0,2,1:T(8,128)(2,1)} %bitcast), channel_id=1, source_target_pairs={{0,1},{1,2},{2,3},{3,4},{4,5},{5,6},{6,7},{7,8},{8,9},{9,10},{10,1... | collective-permute-start | bytes 196616 | tf_op jit(solution)/shard_map/ppermute | solution.py:13
  253.5 5.6 %copy-start.5 = (f32[128,2]{0,1:T(2,128)S(1)}, f32[128,2]{0,1:T(2,128)}, u32[]{:S(2)}) copy-start(f32[128,2]{0,1:T(2,128)} %param.28) | copy-start | bytes 3076
  264.1 2.0 copy-start.2
  307.1 32.9 %all-to-all-start.2 = ((bf16[16,18,2048]{2,1,0:T(8,128)(2,1)}), bf16[16,18,2048]{2,1,0:T(8,128)(2,1)S(1)}, u32[]{:S(2)}, u32[]{:S(2)}) async-start(bf16[16,18,2048]{2,1,0:T(8,128)(2,1)} %bitcast.139), calls=%async_computation.3 | async-start | bytes 3145728 | tf_op jit(solution)/shard_map/all_to_all | solution.py:144
  313.9 4.1 %copy-start.7 = (bf16[1024,2048]{1,0:T(8,128)(2,1)S(1)}, bf16[1024,2048]{1,0:T(8,128)(2,1)}, u32[]{:S(2)}) copy-start(bf16[1024,2048]{1,0:T(8,128)(2,1)} %param.24) | copy-start | bytes 12582916
Sparse Core Ops, SparseCore 0:
  239.8 67.3 reduce-scatter.1
